TPU v7x, 32 devices: a whole 2x2x4 slice. The times are simulated.
32 devices in a mesh: fs: 8 (over z, y), tp: 4 (over x, core).
Axes of the slice: x: 2, y: 2, z: 4, core: 2. Of those that a mesh axis runs over, the one named last changes fastest.
Arguments:
- stream: bfloat16 [3072, 2048], P('fs', 'tp'), may hold values from -3 to 3
- gain_first: float32 [2048], replicated, may hold values from 0.1 to 1.9
- gain_mixer: float32 [2048], replicated, may hold values from 0.1 to 1.9
- gain_second: float32 [2048], replicated, may hold values from 0.1 to 1.9
- gate_weight: float32 [2048, 5632], P('fs', 'tp'), may hold values from -0.125 to 0.125
- gate_scale: float32 [5632], P('tp'), may hold values from 0.5 to 2
- up_weight: float32 [2048, 5632], P('fs', 'tp'), may hold values from -0.125 to 0.125
- up_scale: float32 [5632], P('tp'), may hold values from 0.5 to 2
- down_weight: float32 [5632, 2048], P('tp', 'fs'), may hold values from -0.109375 to 0.109375
- down_scale: float32 [2048], P('tp'), may hold values from 0.5 to 2
- pool_in_weight: float32 [2048, 512], P('fs', 'tp'), may hold values from -0.125 to 0.125
- pool_in_scale: float32 [512], P('tp'), may hold values from 0.5 to 2
- pool_out_weight: float32 [512, 2048], P('tp', 'fs'), may hold values from -0.375 to 0.375
- pool_out_scale: float32 [2048], P('tp'), may hold values from 0.5 to 2
Outputs:
- layer_out: bfloat16 [3072, 2048], P('fs', 'tp')
All inputs are finite; a program needn't handle non-finite values.
Results may differ from a plain program's by a relative error of at most 0.025.
Values may be sent and summed in bfloat16 or wider, within the bound.
A program may use at most 64 MiB of HBM per device.

v0:
```python
import jax
import jax.numpy as jnp
from jax import lax
from jax.sharding import PartitionSpec as P

SEQ = 128
eps = 1e-06
WINDOWS = (2, 4, 8, 16)


def normed(own_columns, norm_gain):
    gathered = lax.all_gather(own_columns, "tp", axis=1, tiled=True)
    floats = gathered.astype(jnp.float32)
    scaled = floats * lax.rsqrt(jnp.mean(floats * floats, axis=-1, keepdims=True) + eps)
    return (scaled * norm_gain).astype(jnp.bfloat16)


def residual_add(own_columns, partial_value, column_scale, factor):
    summed = lax.psum_scatter(
        partial_value.astype(jnp.bfloat16), "tp", scatter_dimension=1, tiled=True
    ).astype(jnp.float32)
    return (own_columns.astype(jnp.float32) + factor * (summed * column_scale)).astype(jnp.bfloat16)


def pooling(pool_input):
    channels = pool_input.shape[1]
    floats = pool_input.astype(jnp.float32).reshape(-1, SEQ, channels)
    csum = jnp.concatenate(
        [jnp.zeros((floats.shape[0], 1, channels), jnp.float32), jnp.cumsum(floats, axis=1)], axis=1
    )
    position = jnp.arange(SEQ)
    channel_index = lax.axis_index("tp") * channels + jnp.arange(channels, dtype=jnp.int32)
    channel_group = channel_index * 4 // (channels * lax.axis_size("tp"))
    pooled = -floats
    for group_index, window in enumerate(WINDOWS):
        before = window // 2
        after_span = window - before
        upper_sum = jnp.pad(csum, ((0, 0), (0, after_span), (0, 0)), mode="edge")[
            :, after_span : after_span + SEQ
        ]
        lower_sum = jnp.pad(csum, ((0, 0), (before, 0), (0, 0)), mode="edge")[:, :SEQ]
        counts = (
            jnp.minimum(position + after_span, SEQ) - jnp.maximum(position - before, 0)
        ).astype(jnp.float32)
        window_mean = (upper_sum - lower_sum) / counts[None, :, None]
        select = (channel_group == group_index).astype(jnp.float32)
        pooled = pooled + window_mean * select
    return pooled.reshape(-1, channels).astype(jnp.bfloat16)


def body(
    stream,
    gain_first,
    gain_mixer,
    gain_second,
    gate_weight,
    gate_scale,
    up_weight,
    up_scale,
    down_weight,
    down_scale,
    pool_in_weight,
    pool_in_scale,
    pool_out_weight,
    pool_out_scale,
):
    gate_half = gate_weight.astype(jnp.bfloat16)
    up_half = up_weight.astype(jnp.bfloat16)
    down_half = down_weight.astype(jnp.bfloat16)
    in_half = pool_in_weight.astype(jnp.bfloat16)
    out_half = pool_out_weight.astype(jnp.bfloat16)
    in_whole, out_whole = (
        lax.all_gather(in_half, "fs", axis=0, tiled=True),
        lax.all_gather(out_half, "fs", axis=1, tiled=True),
    )
    gate_whole, up_whole, down_whole = (
        lax.all_gather(gate_half, "fs", axis=0, tiled=True),
        lax.all_gather(up_half, "fs", axis=0, tiled=True),
        lax.all_gather(down_half, "fs", axis=1, tiled=True),
    )

    def feed_forward(normed_rows):
        gate_sum = jnp.dot(normed_rows, gate_whole, preferred_element_type=jnp.float32) * gate_scale
        up_sum = jnp.dot(normed_rows, up_whole, preferred_element_type=jnp.float32) * up_scale
        hidden = (jax.nn.silu(gate_sum) * up_sum).astype(jnp.bfloat16)
        return jnp.dot(hidden, down_whole, preferred_element_type=jnp.float32)

    after_first = residual_add(stream, feed_forward(normed(stream, gain_first)), down_scale, 0.5)
    mixer_normed = normed(after_first, gain_mixer)
    pool_input = (
        jnp.dot(mixer_normed, in_whole, preferred_element_type=jnp.float32) * pool_in_scale
    ).astype(jnp.bfloat16)
    pooled = pooling(pool_input)
    tp_count = lax.axis_size("tp")
    all_pooled = lax.all_gather(pooled, "tp", axis=1, tiled=True)
    out_columns = lax.all_to_all(out_whole, "tp", split_axis=1, concat_axis=0, tiled=True)
    block_width = out_columns.shape[0] // tp_count
    pooled_blocks = all_pooled.reshape(all_pooled.shape[0], tp_count, block_width)
    weight_blocks = out_columns.reshape(tp_count, block_width, out_columns.shape[1])
    partials = jnp.einsum(
        "rbc,bcd->brd", pooled_blocks, weight_blocks, preferred_element_type=jnp.float32
    ).astype(jnp.bfloat16)
    mixed = jnp.sum(partials.astype(jnp.float32), axis=0)
    after_mix = (after_first.astype(jnp.float32) + mixed * pool_out_scale).astype(jnp.bfloat16)
    return residual_add(after_mix, feed_forward(normed(after_mix, gain_second)), down_scale, 0.5)


def solution(mesh):
    placed = (
        P("fs", "tp"),
        P(),
        P(),
        P(),
        P("fs", "tp"),
        P("tp"),
        P("fs", "tp"),
        P("tp"),
        P("tp", "fs"),
        P("tp"),
        P("fs", "tp"),
        P("tp"),
        P("tp", "fs"),
        P("tp"),
    )
    return jax.shard_map(body, mesh=mesh, in_specs=placed, out_specs=P("fs", "tp"), check_vma=False)
```

profile of v0, /device:TPU:0, one launch (start us, length us, event | category | flops | bytes accessed | tf_op | source)
XLA Modules:
  0.0 509.7 jit_solution(2998391872795220859)
XLA Ops:
  6.5 0.0 all-gather.7.cloned.1.call-start
  6.5 0.7 all-gather.7.cloned.1.call-update
  7.3 0.0 all-gather.9.cloned.1.call-start
  7.3 2.3 convert_element_type.144
  9.6 0.0 all-gather.9.cloned.1.call-update
  9.6 0.0 all-gather.11.cloned.1.call-start
  9.7 0.0 copy-done.5
  9.7 1.0 convert_element_type.145
  10.7 0.0 all-gather.11.cloned.1.call-update
  10.7 0.0 copy-start.11
  10.7 0.0 copy-start.13
  10.7 0.0 all-gather.13.cloned.1.call-start
  10.8 0.5 copy-done.6
  11.2 1.0 convert_element_type.147
  12.2 0.0 all-gather.13.cloned.1.call-update
  12.2 0.0 reduce-scatter.3.cloned.1.call-start
  12.3 19.0 %all-gather.7.cloned.1.call-done = bf16[384,2048]{1,0:T(8,128)(2,1)} async-done(((bf16[384,512]{1,0:T(8,128)(2,1)}), bf16[384,2048]{1,0:T(8,128)(2,1)}) %all-gather.7.cloned.1.call-update) | async-done | bytes 1572880 | tf_op jit(solution)/shard_map/all_gather | solution.py:12
  31.3 1.8 fusion
  33.1 0.0 copy-start.14
  33.1 92.7 %all-gather.9.cloned.1.call-done = bf16[2048,1408]{1,0:T(8,128)(2,1)} async-done(((bf16[256,1408]{1,0:T(8,128)(2,1)}), bf16[2048,1408]{1,0:T(8,128)(2,1)}) %all-gather.9.cloned.1.call-update) | async-done | bytes 5767184 | tf_op jit(solution)/shard_map/all_gather | solution.py:77
  125.8 0.0 copy-done.11
  125.8 0.0 copy-done.13
  125.8 7.1 %convolution_multiply_fusion.3 = f32[384,1408]{1,0:T(8,128)} fusion(bf16[2048,1408]{1,0:T(8,128)(2,1)} %all-gather.9.cloned.1.call-done, f32[1408]{0:T(1024)S(1)} %copy-done.13, bf16[384,2048]{1,0:T(8,128)(2,1)} %all-gather.7.cloned.1.call-done, f32[2048]{0:T(1024)S(1)} %copy-done.11, f32[384]{0:T(512)S(1)} %add_rsqrt_fusion.2), kind=kOutput, calls=%fused_computation.21 | convolution fusion | flops 2218278912 | bytes 9518080 | tf_op jit(solution)/shard_map/dot_general | solution.py:83
  133.0 85.6 %all-gather.11.cloned.1.call-done = bf16[2048,1408]{1,0:T(8,128)(2,1)} async-done(((bf16[256,1408]{1,0:T(8,128)(2,1)}), bf16[2048,1408]{1,0:T(8,128)(2,1)}) %all-gather.11.cloned.1.call-update) | async-done | bytes 5767184 | tf_op jit(solution)/shard_map/all_gather | solution.py:78
  218.5 93.2 %all-gather.13.cloned.1.call-done = bf16[1408,2048]{1,0:T(8,128)(2,1)} async-done(((bf16[1408,256]{1,0:T(8,128)(2,1)}), bf16[1408,2048]{1,0:T(8,128)(2,1)}) %all-gather.13.cloned.1.call-update) | async-done | bytes 5767184 | tf_op jit(solution)/shard_map/all_gather | solution.py:79
  311.8 0.0 copy-done.2
  311.8 0.0 copy-done.14
  311.8 11.2 %convolution_convert_fusion.1 = bf16[384,2048]{1,0:T(8,128)(2,1)} fusion(bf16[1408,2048]{1,0:T(8,128)(2,1)} %all-gather.13.cloned.1.call-done, bf16[2048,1408]{1,0:T(8,128)(2,1)} %all-gather.11.cloned.1.call-done, f32[384,1408]{1,0:T(8,128)} %convolution_multiply_fusion.3, f32[1408]{0:T(1024)S(1)} %copy-done.14, bf16[384,2048]{1,0:T(8,128)(2,1)S(1)} %copy-done.2, ...), kind=kOutput, calls=%fused_computation.23 | convolution fusion | flops 4436901888 | bytes 16858112 | tf_op jit(solution)/shard_map/dot_general | solution.py:86
  323.0 0.0 reduce-scatter.3.cloned.1.call-update
  323.0 0.0 copy-start.8
  323.0 0.0 all-gather.15.cloned.1.call-start
  323.1 26.3 %reduce-scatter.3.cloned.1.call-done = bf16[384,512]{1,0:T(8,128)(2,1)} async-done(((bf16[384,2048]{1,0:T(8,128)(2,1)}), bf16[384,512]{1,0:T(8,128)(2,1)}) %reduce-scatter.3.cloned.1.call-update) | async-done | bytes 393232 | tf_op jit(solution)/shard_map/reduce_scatter | solution.py:19
  349.3 0.0 copy-done.4
  349.3 1.9 add_convert_fusion.2
  351.2 0.0 all-gather.15.cloned.1.call-update
  351.3 0.1 copy.16
  351.4 31.7 %all_gather.34 = bf16[128,2048]{0,1:T(8,128)(2,1)S(1)} all-gather(bf16[128,256]{0,1:T(8,128)(2,1)S(1)} %copy.16), channel_id=1, replica_groups=mesh['fs'=8,'tp'=4] {'fs'}, dimensions={1}, use_global_device_ids=true | all-gather | bytes 589824 | tf_op jit(solution)/shard_map/all_gather | solution.py:74
  383.1 1.0 copy.17
  384.1 3.5 all-to-all-start
  387.6 0.0 all-gather.17.cloned.1.call-start
  387.8 31.5 %all_gather.32 = bf16[2048,128]{1,0:T(8,128)(2,1)S(1)} all-gather(bf16[256,128]{1,0:T(8,128)(2,1)S(1)} %convert_element_type.154), channel_id=1, replica_groups=mesh['fs'=8,'tp'=4] {'fs'}, dimensions={0}, use_global_device_ids=true | all-gather | bytes 589824 | tf_op jit(solution)/shard_map/all_gather | solution.py:73
  419.3 1.8 fusion.3
  421.1 0.0 copy-done.12
  421.1 2.0 fusion.20
  423.2 0.0 copy-start
  423.2 0.0 copy-start.10
  423.2 0.2 reduce_window_sum.11
  423.5 0.3 fusion.46
  423.8 0.1 copy.15
  423.9 6.7 %all_gather.33 = bf16[384,512]{0,1:T(8,128)(2,1)S(1)} all-gather(bf16[384,128]{0,1:T(8,128)(2,1)S(1)} %copy.15), channel_id=1, replica_groups=mesh['fs'=8,'tp'=4] {'tp'}, dimensions={1}, use_global_device_ids=true | all-gather | bytes 491520 | tf_op jit(solution)/shard_map/all_gather | solution.py:95
  430.6 0.0 all-to-all-done
  430.6 0.6 convert_reduce_fusion
  431.2 0.0 copy-start.15
  431.2 0.9 add_convert_fusion.1
  432.1 0.0 all-gather.17.cloned.1.call-update
  432.1 0.2 reduce-scatter.5.cloned.1.call-start
  432.4 20.1 %all-gather.17.cloned.1.call-done = bf16[384,2048]{1,0:T(8,128)(2,1)} async-done(((bf16[384,512]{1,0:T(8,128)(2,1)}), bf16[384,2048]{1,0:T(8,128)(2,1)}) %all-gather.17.cloned.1.call-update) | async-done | bytes 1572880 | tf_op jit(solution)/shard_map/all_gather | solution.py:12
  452.4 1.8 fusion.6
  454.3 7.2 %convolution_multiply_fusion.1 = f32[384,1408]{1,0:T(8,128)} fusion(bf16[2048,1408]{1,0:T(8,128)(2,1)} %all-gather.9.cloned.1.call-done, f32[1408]{0:T(1024)S(1)} %copy-done.13, bf16[384,2048]{1,0:T(8,128)(2,1)} %all-gather.17.cloned.1.call-done, f32[2048]{0:T(1024)S(1)} %copy-done.15, f32[384]{0:T(512)S(1)} %add_rsqrt_fusion), kind=kOutput, calls=%fused_computation.18 | convolution fusion | flops 2218278912 | bytes 9518080 | tf_op jit(solution)/shard_map/dot_general | solution.py:83
  461.5 11.3 %convolution_convert_fusion = bf16[384,2048]{1,0:T(8,128)(2,1)} fusion(bf16[1408,2048]{1,0:T(8,128)(2,1)} %all-gather.13.cloned.1.call-done, bf16[2048,1408]{1,0:T(8,128)(2,1)} %all-gather.11.cloned.1.call-done, f32[384,1408]{1,0:T(8,128)} %convolution_multiply_fusion.1, f32[1408]{0:T(1024)S(1)} %copy-done.14, bf16[384,2048]{1,0:T(8,128)(2,1)S(1)} %copy-done.3, ...), kind=kOutput, calls=%fused_computation.22 | convolution fusion | flops 4436901888 | bytes 16858112 | tf_op jit(solution)/shard_map/dot_general | solution.py:86
  472.8 0.0 reduce-scatter.5.cloned.1.call-update
  472.8 28.1 %reduce-scatter.5.cloned.1.call-done = bf16[384,512]{1,0:T(8,128)(2,1)} async-done(((bf16[384,2048]{1,0:T(8,128)(2,1)}), bf16[384,512]{1,0:T(8,128)(2,1)}) %reduce-scatter.5.cloned.1.call-update) | async-done | bytes 393232 | tf_op jit(solution)/shard_map/reduce_scatter | solution.py:19
  501.0 0.0 copy-done.1
  501.0 1.9 add_convert_fusion
  (38 shorter events, 0.2 us)
Async XLA Ops:
  6.5 3.2 copy-start.5
  6.5 24.7 %all-gather.7.cloned.1.call-start = ((), (), s32[]{:S(2)}) async-start(), calls=%async_computation.3 | async-start | bytes 1966080 | tf_op jit(solution)/shard_map/all_gather | solution.py:12
  7.3 118.5 %all-gather.9.cloned.1.call-start = ((), (), s32[]{:S(2)}) async-start(), calls=%async_computation.4 | async-start | bytes 6488064 | tf_op jit(solution)/shard_map/all_gather | solution.py:77
  9.6 1.6 copy-start.6
  9.6 208.9 %all-gather.11.cloned.1.call-start = ((), (), s32[]{:S(2)}) async-start(), calls=%async_computation.5 | async-start | bytes 6488064 | tf_op jit(solution)/shard_map/all_gather | solution.py:78
  10.7 115.1 %copy-start.11 = (f32[2048]{0:T(1024)S(1)}, f32[2048]{0:T(1024)}, u32[]{:S(2)}) copy-start(f32[2048]{0:T(1024)} %param.15) | copy-start | bytes 24580
  10.7 115.1 %copy-start.13 = (f32[1408]{0:T(1024)S(1)}, f32[1408]{0:T(1024)}, u32[]{:S(2)}) copy-start(f32[1408]{0:T(1024)} %param.19) | copy-start | bytes 16900
  10.7 301.1 %all-gather.13.cloned.1.call-start = ((), (), s32[]{:S(2)}) async-start(), calls=%async_computation.6 | async-start | bytes 6488064 | tf_op jit(solution)/shard_map/all_gather | solution.py:79
  12.2 337.1 %reduce-scatter.3.cloned.1.call-start = ((), (), s32[]{:S(2)}) async-start(), calls=%async_computation.7 | async-start | bytes 1966080 | tf_op jit(solution)/shard_map/reduce_scatter | solution.py:19
  33.1 278.7 %copy-start.2 = (bf16[384,2048]{1,0:T(8,128)(2,1)S(1)}, bf16[384,2048]{1,0:T(8,128)(2,1)}, u32[]{:S(2)}) copy-start(bf16[384,2048]{1,0:T(8,128)(2,1)} %all-gather.7.cloned.1.call-done) | copy-start | bytes 4718596
  33.1 278.7 %copy-start.14 = (f32[1408]{0:T(1024)S(1)}, f32[1408]{0:T(1024)}, u32[]{:S(2)}) copy-start(f32[1408]{0:T(1024)} %param.21) | copy-start | bytes 16900
  133.0 216.4 %copy-start.4 = (bf16[384,512]{1,0:T(8,128)(2,1)S(1)}, bf16[384,512]{1,0:T(8,128)(2,1)}, u32[]{:S(2)}) copy-start(bf16[384,512]{1,0:T(8,128)(2,1)} %param.14) | copy-start | bytes 1179652
  133.0 216.4 %copy-start.9 = (f32[512]{0:T(512)S(1)}, f32[512]{0:T(512)}, u32[]{:S(2)}) copy-start(f32[512]{0:T(512)} %param.23) | copy-start | bytes 6148
  323.0 28.3 %copy-start.7 = (f32[128,256]{1,0:T(8,128)S(1)}, f32[128,256]{1,0:T(8,128)}, u32[]{:S(2)}) copy-start(f32[128,256]{1,0:T(8,128)} %param.26) | copy-start | bytes 393220
  323.0 64.6 %copy-start.8 = (f32[256,128]{1,0:T(8,128)S(1)}, f32[256,128]{1,0:T(8,128)}, u32[]{:S(2)}) copy-start(f32[256,128]{1,0:T(8,128)} %param.24) | copy-start | bytes 393220
  323.0 96.3 %all-gather.15.cloned.1.call-start = ((), (), s32[]{:S(2)}) async-start(), calls=%async_computation.8 | async-start | bytes 1966080 | tf_op jit(solution)/shard_map/all_gather | solution.py:12
  383.1 38.0 %copy-start.12 = (f32[2048]{0:T(1024)S(1)}, f32[2048]{0:T(1024)}, u32[]{:S(2)}) copy-start(f32[2048]{0:T(1024)} %param.16) | copy-start | bytes 24580
  383.1 38.0 %copy-start.16 = (f32[128]{0:T(128)S(1)}, f32[128]{0:T(128)}, u32[]{:S(2)}) copy-start(f32[128]{0:T(128)} %param.25) | copy-start | bytes 1540
  384.1 46.5 %all-to-all-start = ((bf16[128,4,512]{2,0,1:T(8,128)(2,1)}), bf16[128,4,512]{2,0,1:T(8,128)(2,1)S(1)}, u32[]{:S(2)}, u32[]{:S(2)}) async-start(bf16[128,4,512]{2,0,1:T(8,128)(2,1)} %copy.17), calls=%async_computation.1 | async-start | bytes 1048576 | tf_op jit(solution)/shard_map/all_to_all | solution.py:96
  387.6 64.9 %all-gather.17.cloned.1.call-start = ((), (), s32[]{:S(2)}) async-start(), calls=%async_computation.9 | async-start | bytes 1966080 | tf_op jit(solution)/shard_map/all_gather | solution.py:12
  423.2 8.0 %copy-start = (bf16[384,512]{1,0:T(8,128)(2,1)S(1)}, bf16[384,512]{1,0:T(8,128)(2,1)}, u32[]{:S(2)}) copy-start(bf16[384,512]{1,0:T(8,128)(2,1)} %add_convert_fusion.2) | copy-start | bytes 1179652
  423.2 8.0 %copy-start.10 = (f32[512]{0:T(512)S(1)}, f32[512]{0:T(512)}, u32[]{:S(2)}) copy-start(f32[512]{0:T(512)} %param.27) | copy-start | bytes 6148
  431.2 23.0 %copy-start.15 = (f32[2048]{0:T(1024)S(1)}, f32[2048]{0:T(1024)}, u32[]{:S(2)}) copy-start(f32[2048]{0:T(1024)} %param.17) | copy-start | bytes 24580
  432.1 68.8 %reduce-scatter.5.cloned.1.call-start = ((), (), s32[]{:S(2)}) async-start(), calls=%async_computation.10 | async-start | bytes 1966080 | tf_op jit(solution)/shard_map/reduce_scatter | solution.py:19
  454.3 7.3 %copy-start.3 = (bf16[384,2048]{1,0:T(8,128)(2,1)S(1)}, bf16[384,2048]{1,0:T(8,128)(2,1)}, u32[]{:S(2)}) copy-start(bf16[384,2048]{1,0:T(8,128)(2,1)} %all-gather.17.cloned.1.call-done) | copy-start | bytes 4718596
  461.5 39.4 %copy-start.1 = (bf16[384,512]{1,0:T(8,128)(2,1)S(1)}, bf16[384,512]{1,0:T(8,128)(2,1)}, u32[]{:S(2)}) copy-start(bf16[384,512]{1,0:T(8,128)(2,1)} %add_convert_fusion.1) | copy-start | bytes 1179652
Sparse Core Ops, SparseCore 0:
  8.9 22.3 all-gather.6
  33.5 92.2 all-gather.8
  128.0 90.4 all-gather.10
  220.4 91.2 all-gather.12
  323.1 26.1 reduce-scatter.2
  351.4 19.6 all-gather.14
  432.3 20.1 all-gather.16
  472.9 27.9 reduce-scatter.4
where the time goes:
time: 510 us
  waiting for transfers between devices  366 us (72%)
  blocking collectives  69.9 us (14%)
  matrix products  39.5 us (8%)
  other arithmetic  14.9 us (3%)
  between operations  13.8 us (3%)
    all_gather x1, waiting for transfers between devices, body(): lax.all_gather(down_half, 'fs', axis=1, tiled=True)  93.2 us
    all_gather x1, waiting for transfers between devices, body(): lax.all_gather(gate_half, 'fs', axis=0, tiled=True)  92.7 us
    all_gather x1, waiting for transfers between devices, body(): lax.all_gather(up_half, 'fs', axis=0, tiled=True)  85.6 us
    reduce_scatter x2, waiting for transfers between devices, residual_add(): lax.psum_scatter(partial_value.astype(jnp.bfloat16), 'tp', scatter_dimens...  54.4 us
    all_gather x3, waiting for transfers between devices, normed(): gathered = lax.all_gather(own_columns, 'tp', axis=1, tiled=True)  39.1 us
    all_gather x1, blocking collectives, body(): lax.all_gather(out_half, 'fs', axis=1, tiled=True)  31.7 us
    all_gather x1, blocking collectives, body(): lax.all_gather(in_half, 'fs', axis=0, tiled=True)  31.5 us
    dot_general x2, matrix products, feed_forward(): return jnp.dot(hidden, down_whole, preferred_element_type=jnp.float32)  22.5 us
  transfers between devices with their start and end apart: 9, of which 7 were waited for; matrix products, arithmetic and copies ran while one was open for 4% of the time, Pallas kernels for 0%

commit v1 on v0

--- a/solution.py
+++ b/solution.py
@@ -1,11 +1,22 @@
+import functools
 import jax
 import jax.numpy as jnp
 from jax import lax
 from jax.sharding import PartitionSpec as P
+from jax.lax import all_gather
 
 SEQ = 128
 eps = 1e-06
 WINDOWS = (2, 4, 8, 16)
+
+
+def move_state_in(vec, mesh_ax, which_dim):
+    left_arr = all_gather(vec, axis_name=mesh_ax)
+    t1 = jnp.concatenate(left_arr, which_dim)
+    return t1
+
+
+advance_lanes = functools.partial(move_state_in, mesh_ax="fs", which_dim=1)
 
 
 def normed(own_columns, norm_gain):
@@ -76,7 +87,7 @@
     gate_whole, up_whole, down_whole = (
         lax.all_gather(gate_half, "fs", axis=0, tiled=True),
         lax.all_gather(up_half, "fs", axis=0, tiled=True),
-        lax.all_gather(down_half, "fs", axis=1, tiled=True),
+        advance_lanes(down_half),
     )
 
     def feed_forward(normed_rows):

time: 510 us -> 510 us (level)
  waiting for transfers between devices: 366 us -> 357 us
  local copies, waits for them, and re-layouts: 1.86 us -> 10.1 us
    all_gather x1, waiting for transfers between devices: 92.7 us -> 84.4 us  [body(): lax.all_gather(gate_half, 'fs', axis=0, tiled=True)]
    reshape x0 -> x1, local copies, waits for them, and re-layouts: none -> 8.3 us  [move_state_in(): t1 = jnp.concatenate(left_arr, which_dim)]
  transfers between devices with their start and end apart: 9 -> 9, of which waited for: 7 -> 7; matrix products, arithmetic and copies ran while one was open for 4% -> 5% of each run, Pallas kernels for 0% -> 0%
where the time goes in v1:
time: 510 us; the launch traced here: 509 us
  waiting for transfers between devices  357 us (70%)
  blocking collectives  69.9 us (14%)
  matrix products  39 us (8%)
  other arithmetic  14.9 us (3%)
  between operations  13.8 us (3%)
  local copies, waits for them, and re-layouts  10.1 us (2%)
    all_gather x1, waiting for transfers between devices, move_state_in(): left_arr = all_gather(vec, axis_name=mesh_ax)  92.7 us
    all_gather x1, waiting for transfers between devices, body(): lax.all_gather(up_half, 'fs', axis=0, tiled=True)  85.9 us
    all_gather x1, waiting for transfers between devices, body(): lax.all_gather(gate_half, 'fs', axis=0, tiled=True)  84.4 us
    reduce_scatter x2, waiting for transfers between devices, residual_add(): lax.psum_scatter(partial_value.astype(jnp.bfloat16), 'tp', scatter_dimens...  54.4 us
    all_gather x3, waiting for transfers between devices, normed(): gathered = lax.all_gather(own_columns, 'tp', axis=1, tiled=True)  39.1 us
    all_gather x1, blocking collectives, body(): lax.all_gather(out_half, 'fs', axis=1, tiled=True)  31.7 us
    all_gather x1, blocking collectives, body(): lax.all_gather(in_half, 'fs', axis=0, tiled=True)  31.5 us
    dot_general x2, matrix products, feed_forward(): return jnp.dot(hidden, down_whole, preferred_element_type=jnp.float32)  22.5 us
  transfers between devices with their start and end apart: 9, of which 7 were waited for; matrix products, arithmetic and copies ran while one was open for 5% of the time, Pallas kernels for 0%

profile of v1, /device:TPU:0, one launch (start us, length us, event | category | flops | bytes accessed | tf_op | source)
XLA Modules:
  0.0 509.0 jit_solution(758110273829904852)
XLA Ops:
  6.5 0.0 all-gather.8.cloned.1.call-start
  6.5 0.7 all-gather.8.cloned.1.call-update
  7.3 0.0 all-gather.18.cloned.1.call-start
  7.3 2.3 convert_element_type.147
  9.6 0.0 all-gather.18.cloned.1.call-update
  9.6 0.0 all-gather.10.cloned.1.call-start
  9.7 0.0 copy-done.5
  9.7 1.0 convert_element_type.144
  10.7 0.0 all-gather.10.cloned.1.call-update
  10.7 0.0 all-gather.12.cloned.1.call-start
  10.8 0.5 copy-done.6
  11.2 1.0 convert_element_type.145
  12.2 0.0 all-gather.12.cloned.1.call-update
  12.3 0.0 reduce-scatter.3.cloned.1.call-start
  12.3 19.0 %all-gather.8.cloned.1.call-done = bf16[384,2048]{1,0:T(8,128)(2,1)} async-done(((bf16[384,512]{1,0:T(8,128)(2,1)}), bf16[384,2048]{1,0:T(8,128)(2,1)}) %all-gather.8.cloned.1.call-update) | async-done | bytes 1572880 | tf_op jit(solution)/shard_map/all_gather | solution.py:23
  31.3 1.8 fusion
  33.1 92.7 %all-gather.18.cloned.1.call-done = bf16[11264,256]{1,0:T(8,128)(2,1)} async-done(((bf16[1408,256]{1,0:T(8,128)(2,1)}), bf16[11264,256]{1,0:T(8,128)(2,1)}) %all-gather.18.cloned.1.call-update) | async-done | bytes 5767184 | tf_op jit(solution)/shard_map/all_gather | solution.py:14
  125.8 8.3 %copy.19 = bf16[1408,8,256]{0,2,1:T(8,128)(2,1)} copy(bf16[1408,8,256]{2,0,1:T(8,128)(2,1)} %bitcast.25) | data formatting | bytes 11534336 | tf_op jit(solution)/shard_map/reshape | solution.py:15
  134.1 84.4 %all-gather.10.cloned.1.call-done = bf16[2048,1408]{1,0:T(8,128)(2,1)} async-done(((bf16[256,1408]{1,0:T(8,128)(2,1)}), bf16[2048,1408]{1,0:T(8,128)(2,1)}) %all-gather.10.cloned.1.call-update) | async-done | bytes 5767184 | tf_op jit(solution)/shard_map/all_gather | solution.py:88
  218.5 0.0 copy-done.2
  218.5 0.0 copy-done.11
  218.5 6.7 %convolution_multiply_fusion.3 = f32[384,1408]{1,0:T(8,128)} fusion(bf16[2048,1408]{1,0:T(8,128)(2,1)} %all-gather.10.cloned.1.call-done, f32[1408]{0:T(1024)S(1)} %copy-done.13, bf16[384,2048]{1,0:T(8,128)(2,1)S(1)} %copy-done.2, f32[2048]{0:T(1024)S(1)} %copy-done.11, f32[384]{0:T(512)S(1)} %add_rsqrt_fusion.2), kind=kOutput, calls=%fused_computation.21 | convolution fusion | flops 2218278912 | bytes 9518080 | tf_op jit(solution)/shard_map/dot_general | solution.py:94
  225.2 85.9 %all-gather.12.cloned.1.call-done = bf16[2048,1408]{1,0:T(8,128)(2,1)} async-done(((bf16[256,1408]{1,0:T(8,128)(2,1)}), bf16[2048,1408]{1,0:T(8,128)(2,1)}) %all-gather.12.cloned.1.call-update) | async-done | bytes 5767184 | tf_op jit(solution)/shard_map/all_gather | solution.py:89
  311.1 11.3 %convolution_convert_fusion.1 = bf16[384,2048]{1,0:T(8,128)(2,1)} fusion(bf16[1408,2048]{0,1:T(8,128)(2,1)} %bitcast.23, bf16[2048,1408]{1,0:T(8,128)(2,1)} %all-gather.12.cloned.1.call-done, f32[384,1408]{1,0:T(8,128)} %convolution_multiply_fusion.3, f32[1408]{0:T(1024)S(1)} %copy-done.14, bf16[384,2048]{1,0:T(8,128)(2,1)S(1)} %copy-done.2, ...), kind=kOutput, calls=%fused_computation.23 | convolution fusion | flops 4436901888 | bytes 16858112 | tf_op jit(solution)/shard_map/dot_general | solution.py:97
  322.3 0.0 reduce-scatter.3.cloned.1.call-update
  322.4 0.0 copy-start.8
  322.4 0.0 all-gather.14.cloned.1.call-start
  322.4 26.3 %reduce-scatter.3.cloned.1.call-done = bf16[384,512]{1,0:T(8,128)(2,1)} async-done(((bf16[384,2048]{1,0:T(8,128)(2,1)}), bf16[384,512]{1,0:T(8,128)(2,1)}) %reduce-scatter.3.cloned.1.call-update) | async-done | bytes 393232 | tf_op jit(solution)/shard_map/reduce_scatter | solution.py:30
  348.7 0.0 copy-done.4
  348.7 1.9 add_convert_fusion.2
  350.6 0.0 all-gather.14.cloned.1.call-update
  350.6 0.0 copy-done.7
  350.6 0.1 copy.21
  350.7 31.7 %all_gather.38 = bf16[128,2048]{0,1:T(8,128)(2,1)S(1)} all-gather(bf16[128,256]{0,1:T(8,128)(2,1)S(1)} %copy.21), channel_id=1, replica_groups=mesh['fs'=8,'tp'=4] {'fs'}, dimensions={1}, use_global_device_ids=true | all-gather | bytes 589824 | tf_op jit(solution)/shard_map/all_gather | solution.py:85
  382.5 1.0 copy.22
  383.5 3.5 all-to-all-start
  387.0 0.0 all-gather.16.cloned.1.call-start
  387.2 31.5 %all_gather.36 = bf16[2048,128]{1,0:T(8,128)(2,1)S(1)} all-gather(bf16[256,128]{1,0:T(8,128)(2,1)S(1)} %convert_element_type.154), channel_id=1, replica_groups=mesh['fs'=8,'tp'=4] {'fs'}, dimensions={0}, use_global_device_ids=true | all-gather | bytes 589824 | tf_op jit(solution)/shard_map/all_gather | solution.py:84
  418.7 1.8 fusion.3
  420.5 0.0 copy-done.12
  420.5 2.0 fusion.20
  422.5 0.0 copy-start
  422.5 0.0 copy-start.10
  422.6 0.2 reduce_window_sum.11
  422.8 0.3 fusion.46
  423.1 0.1 copy.20
  423.3 6.7 %all_gather.37 = bf16[384,512]{0,1:T(8,128)(2,1)S(1)} all-gather(bf16[384,128]{0,1:T(8,128)(2,1)S(1)} %copy.20), channel_id=1, replica_groups=mesh['fs'=8,'tp'=4] {'tp'}, dimensions={1}, use_global_device_ids=true | all-gather | bytes 491520 | tf_op jit(solution)/shard_map/all_gather | solution.py:106
  429.9 0.0 all-to-all-done
  429.9 0.6 convert_reduce_fusion
  430.5 0.0 copy-done
  430.6 0.0 copy-done.10
  430.6 0.0 copy-start.15
  430.6 0.9 add_convert_fusion.1
  431.5 0.0 all-gather.16.cloned.1.call-update
  431.5 0.2 reduce-scatter.5.cloned.1.call-start
  431.7 20.1 %all-gather.16.cloned.1.call-done = bf16[384,2048]{1,0:T(8,128)(2,1)} async-done(((bf16[384,512]{1,0:T(8,128)(2,1)}), bf16[384,2048]{1,0:T(8,128)(2,1)}) %all-gather.16.cloned.1.call-update) | async-done | bytes 1572880 | tf_op jit(solution)/shard_map/all_gather | solution.py:23
  451.8 1.8 fusion.6
  453.6 0.0 copy-done.15
  453.6 0.0 copy-start.3
  453.6 7.2 %convolution_multiply_fusion.1 = f32[384,1408]{1,0:T(8,128)} fusion(bf16[2048,1408]{1,0:T(8,128)(2,1)} %all-gather.10.cloned.1.call-done, f32[1408]{0:T(1024)S(1)} %copy-done.13, bf16[384,2048]{1,0:T(8,128)(2,1)} %all-gather.16.cloned.1.call-done, f32[2048]{0:T(1024)S(1)} %copy-done.15, f32[384]{0:T(512)S(1)} %add_rsqrt_fusion), kind=kOutput, calls=%fused_computation.18 | convolution fusion | flops 2218278912 | bytes 9518080 | tf_op jit(solution)/shard_map/dot_general | solution.py:94
  460.9 11.3 %convolution_convert_fusion = bf16[384,2048]{1,0:T(8,128)(2,1)} fusion(bf16[1408,2048]{0,1:T(8,128)(2,1)} %bitcast.24, bf16[2048,1408]{1,0:T(8,128)(2,1)} %all-gather.12.cloned.1.call-done, f32[384,1408]{1,0:T(8,128)} %convolution_multiply_fusion.1, f32[1408]{0:T(1024)S(1)} %copy-done.14, bf16[384,2048]{1,0:T(8,128)(2,1)S(1)} %copy-done.3, ...), kind=kOutput, calls=%fused_computation.22 | convolution fusion | flops 4436901888 | bytes 16858112 | tf_op jit(solution)/shard_map/dot_general | solution.py:97
  472.1 0.0 reduce-scatter.5.cloned.1.call-update
  472.2 28.2 %reduce-scatter.5.cloned.1.call-done = bf16[384,512]{1,0:T(8,128)(2,1)} async-done(((bf16[384,2048]{1,0:T(8,128)(2,1)}), bf16[384,512]{1,0:T(8,128)(2,1)}) %reduce-scatter.5.cloned.1.call-update) | async-done | bytes 393232 | tf_op jit(solution)/shard_map/reduce_scatter | solution.py:30
  500.3 1.9 add_convert_fusion
  (39 shorter events, 0.2 us)
Async XLA Ops:
  6.5 3.2 copy-start.5
  6.5 24.7 %all-gather.8.cloned.1.call-start = ((), (), s32[]{:S(2)}) async-start(), calls=%async_computation.3 | async-start | bytes 1966080 | tf_op jit(solution)/shard_map/all_gather | solution.py:23
  7.3 118.5 %all-gather.18.cloned.1.call-start = ((), (), s32[]{:S(2)}) async-start(), calls=%async_computation.10 | async-start | bytes 6488064 | tf_op jit(solution)/shard_map/all_gather | solution.py:14
  9.6 1.6 copy-start.6
  9.6 208.9 %all-gather.10.cloned.1.call-start = ((), (), s32[]{:S(2)}) async-start(), calls=%async_computation.4 | async-start | bytes 6488064 | tf_op jit(solution)/shard_map/all_gather | solution.py:88
  10.7 300.4 %all-gather.12.cloned.1.call-start = ((), (), s32[]{:S(2)}) async-start(), calls=%async_computation.5 | async-start | bytes 6488064 | tf_op jit(solution)/shard_map/all_gather | solution.py:89
  12.3 336.4 %reduce-scatter.3.cloned.1.call-start = ((), (), s32[]{:S(2)}) async-start(), calls=%async_computation.6 | async-start | bytes 1966080 | tf_op jit(solution)/shard_map/reduce_scatter | solution.py:30
  125.8 92.7 %copy-start.2 = (bf16[384,2048]{1,0:T(8,128)(2,1)S(1)}, bf16[384,2048]{1,0:T(8,128)(2,1)}, u32[]{:S(2)}) copy-start(bf16[384,2048]{1,0:T(8,128)(2,1)} %all-gather.8.cloned.1.call-done) | copy-start | bytes 4718596
  125.8 92.7 %copy-start.11 = (f32[2048]{0:T(1024)S(1)}, f32[2048]{0:T(1024)}, u32[]{:S(2)}) copy-start(f32[2048]{0:T(1024)} %param.15) | copy-start | bytes 24580
  125.8 92.7 %copy-start.13 = (f32[1408]{0:T(1024)S(1)}, f32[1408]{0:T(1024)}, u32[]{:S(2)}) copy-start(f32[1408]{0:T(1024)} %param.19) | copy-start | bytes 16900
  134.1 177.0 %copy-start.14 = (f32[1408]{0:T(1024)S(1)}, f32[1408]{0:T(1024)}, u32[]{:S(2)}) copy-start(f32[1408]{0:T(1024)} %param.21) | copy-start | bytes 16900
  311.1 37.6 %copy-start.4 = (bf16[384,512]{1,0:T(8,128)(2,1)S(1)}, bf16[384,512]{1,0:T(8,128)(2,1)}, u32[]{:S(2)}) copy-start(bf16[384,512]{1,0:T(8,128)(2,1)} %param.14) | copy-start | bytes 1179652
  311.1 37.6 %copy-start.9 = (f32[512]{0:T(512)S(1)}, f32[512]{0:T(512)}, u32[]{:S(2)}) copy-start(f32[512]{0:T(512)} %param.23) | copy-start | bytes 6148
  322.3 28.3 %copy-start.7 = (f32[128,256]{1,0:T(8,128)S(1)}, f32[128,256]{1,0:T(8,128)}, u32[]{:S(2)}) copy-start(f32[128,256]{1,0:T(8,128)} %param.26) | copy-start | bytes 393220
  322.4 64.7 %copy-start.8 = (f32[256,128]{1,0:T(8,128)S(1)}, f32[256,128]{1,0:T(8,128)}, u32[]{:S(2)}) copy-start(f32[256,128]{1,0:T(8,128)} %param.24) | copy-start | bytes 393220
  322.4 96.3 %all-gather.14.cloned.1.call-start = ((), (), s32[]{:S(2)}) async-start(), calls=%async_computation.7 | async-start | bytes 1966080 | tf_op jit(solution)/shard_map/all_gather | solution.py:23
  382.5 38.0 %copy-start.12 = (f32[2048]{0:T(1024)S(1)}, f32[2048]{0:T(1024)}, u32[]{:S(2)}) copy-start(f32[2048]{0:T(1024)} %param.16) | copy-start | bytes 24580
  382.5 38.0 %copy-start.16 = (f32[128]{0:T(128)S(1)}, f32[128]{0:T(128)}, u32[]{:S(2)}) copy-start(f32[128]{0:T(128)} %param.25) | copy-start | bytes 1540
  383.5 46.4 %all-to-all-start = ((bf16[128,4,512]{2,0,1:T(8,128)(2,1)}), bf16[128,4,512]{2,0,1:T(8,128)(2,1)S(1)}, u32[]{:S(2)}, u32[]{:S(2)}) async-start(bf16[128,4,512]{2,0,1:T(8,128)(2,1)} %copy.22), calls=%async_computation.1 | async-start | bytes 1048576 | tf_op jit(solution)/shard_map/all_to_all | solution.py:107
  387.0 64.9 %all-gather.16.cloned.1.call-start = ((), (), s32[]{:S(2)}) async-start(), calls=%async_computation.8 | async-start | bytes 1966080 | tf_op jit(solution)/shard_map/all_gather | solution.py:23
  422.5 8.0 %copy-start = (bf16[384,512]{1,0:T(8,128)(2,1)S(1)}, bf16[384,512]{1,0:T(8,128)(2,1)}, u32[]{:S(2)}) copy-start(bf16[384,512]{1,0:T(8,128)(2,1)} %add_convert_fusion.2) | copy-start | bytes 1179652
  422.5 8.0 %copy-start.10 = (f32[512]{0:T(512)S(1)}, f32[512]{0:T(512)}, u32[]{:S(2)}) copy-start(f32[512]{0:T(512)} %param.27) | copy-start | bytes 6148
  430.6 23.1 %copy-start.15 = (f32[2048]{0:T(1024)S(1)}, f32[2048]{0:T(1024)}, u32[]{:S(2)}) copy-start(f32[2048]{0:T(1024)} %param.17) | copy-start | bytes 24580
  431.5 68.8 %reduce-scatter.5.cloned.1.call-start = ((), (), s32[]{:S(2)}) async-start(), calls=%async_computation.9 | async-start | bytes 1966080 | tf_op jit(solution)/shard_map/reduce_scatter | solution.py:30
  453.6 7.3 %copy-start.3 = (bf16[384,2048]{1,0:T(8,128)(2,1)S(1)}, bf16[384,2048]{1,0:T(8,128)(2,1)}, u32[]{:S(2)}) copy-start(bf16[384,2048]{1,0:T(8,128)(2,1)} %all-gather.16.cloned.1.call-done) | copy-start | bytes 4718596
  460.9 39.4 %copy-start.1 = (bf16[384,512]{1,0:T(8,128)(2,1)S(1)}, bf16[384,512]{1,0:T(8,128)(2,1)}, u32[]{:S(2)}) copy-start(bf16[384,512]{1,0:T(8,128)(2,1)} %add_convert_fusion.1) | copy-start | bytes 1179652
Sparse Core Ops, SparseCore 0:
  8.9 22.3 all-gather.7
  33.5 92.2 all-gather.17
  128.0 90.4 all-gather.9
  220.6 90.4 all-gather.11
  322.5 26.1 reduce-scatter.2
  350.7 19.6 all-gather.13
  431.6 20.1 all-gather.15
  472.3 27.9 reduce-scatter.4
